TPU v7x, 32 devices: a whole 2x2x4 slice. The times are simulated.
32 devices in a mesh: ep: 8 (over z, x), tp: 4 (over y, core).
Axes of the slice: x: 2, y: 2, z: 4, core: 2. Of those that a mesh axis runs over, the one named last changes fastest.
Arguments:
- mix_bgate: bfloat16 [2048, 1024], P('ep', 'tp'), may hold values from -6 to 6
- mix_cgate: bfloat16 [2048, 1024], P('ep', 'tp'), may hold values from -6 to 6
- mix_input: bfloat16 [2048, 1024], P('ep', 'tp'), may hold values from -6 to 6
- conv_taps: float32 [3, 1024], P(None, 'tp'), may hold values from -3.5 to 3.5
- mix_out_w: bfloat16 [1024, 2048], P('tp'), may hold values from -0.1875 to 0.1875
- moe_x: bfloat16 [2048, 2048], P('ep', 'tp'), may hold values from -6 to 6
- moe_gain: float32 [2048], replicated, may hold values from 0.1 to 1.9
- routes: int32 [2048, 2], P('ep'), may hold values from 0 to 7, all different within a row; in each aligned block of 256 rows (0 to 255, 256 to 511, ...) at most 96 rows name the same one
- route_w: float32 [2048, 2], P('ep'), may hold values from 0.2 to 1
- w_gate: bfloat16 [8, 2048, 3584], P('ep', None, 'tp'), may hold values from -0.125 to 0.125
- w_up: bfloat16 [8, 2048, 3584], P('ep', None, 'tp'), may hold values from -0.125 to 0.125
- w_down: bfloat16 [8, 3584, 2048], P('ep', 'tp'), may hold values from -0.09375 to 0.09375
Outputs:
- mixed: bfloat16 [2048, 2048], P(('ep', 'tp'))
- routed: bfloat16 [2048, 2048], P('ep', 'tp')
Inputs may be any that keep to these rules, and one draw needn't show every extreme that they name: `routes`: among the 256 rows of one index of ep, each row names 2 different experts and no expert is named by more than 96 rows; in every draw some expert is named by exactly 96 rows of some index.
All inputs are finite; a program needn't handle non-finite values.
Results may differ from a plain program's by a relative error of at most 0.012.
Values may be sent and summed in bfloat16 or wider, within the bound.
No kernel may reach another device: no remote copies, remote signals or barrier semaphores. Data moves between devices by JAX's collectives and lax.ppermute only.
A program may use at most 64 MiB of HBM per device.

v0:
```python
import jax
import jax.numpy as jnp
from jax import lax
from jax.sharding import PartitionSpec as P


def shifted(block, axis, distance):
    devices = range(lax.axis_size(axis))
    route = [(i - distance, i) for i in devices if i - distance in devices]
    return lax.ppermute(block, axis, route)


def rms_rows(values, gain):
    wide = values.astype(jnp.float32)
    scale = lax.rsqrt(jnp.mean(wide * wide, axis=-1, keepdims=True) + 1e-06)
    return (wide * scale * gain).astype(jnp.bfloat16)


def conv_mixer(mix_bgate, mix_cgate, mix_input, conv_taps, mix_out_w):
    length = mix_input.shape[0]
    reach = conv_taps.shape[0] - 1
    tail = jnp.stack([mix_cgate[length - reach :], mix_input[length - reach :]])
    before = shifted(tail, "ep", 1)
    gates_c = jnp.concatenate([before[0], mix_cgate], 0).astype(jnp.float32)
    inputs_h = jnp.concatenate([before[1], mix_input], 0).astype(jnp.float32)
    prod = gates_c * inputs_h
    conv = conv_taps[0] * prod[0:length]
    for j in range(1, reach + 1):
        conv = conv + conv_taps[j] * prod[j : j + length]
    gated = (mix_bgate.astype(jnp.float32) * conv).astype(jnp.bfloat16)
    return lax.psum_scatter(
        jnp.dot(gated, mix_out_w, preferred_element_type=jnp.float32).astype(jnp.bfloat16),
        "tp",
        scatter_dimension=0,
        tiled=True,
    )


def expert_layer(moe_x, moe_gain, routes, route_w, w_gate, w_up, w_down):
    whole = lax.all_gather(moe_x, "tp", axis=1, tiled=True)
    normed = rms_rows(whole, moe_gain)
    ntok, width = normed.shape
    top = routes.shape[1]
    n_ep = lax.axis_size("ep")
    n_tp = lax.axis_size("tp")
    per_dev = w_gate.shape[0]
    experts = per_dev * n_ep
    cap = 4 * ((3 * ntok * top + 8 * experts - 1) // (8 * experts))
    flat = routes.reshape(-1)
    onehot = (flat[:, None] == jnp.arange(experts, dtype=jnp.int32)[None, :]).astype(jnp.int32)
    earlier = jnp.cumsum(onehot, axis=0) - onehot
    slot = jnp.sum(earlier * onehot, axis=1)
    place = flat * cap + slot
    source = (
        jnp.full((experts * cap,), ntok, jnp.int32)
        .at[place]
        .set(jnp.arange(ntok * top, dtype=jnp.int32) // top)
    )
    padded = jnp.concatenate([normed, jnp.zeros((1, width), jnp.bfloat16)], 0)
    outgoing = padded[source].reshape(n_ep, per_dev, cap, width)
    part = cap // n_tp
    mine = lax.dynamic_slice_in_dim(outgoing, lax.axis_index("tp") * part, part, 2)
    landed = lax.all_to_all(mine, "ep", split_axis=0, concat_axis=0, tiled=True)
    arrived = lax.all_gather(landed, "tp", axis=2, tiled=True)
    gate = jnp.einsum("secd,edf->secf", arrived, w_gate, preferred_element_type=jnp.float32)
    upper = jnp.einsum("secd,edf->secf", arrived, w_up, preferred_element_type=jnp.float32)
    hidden = (jax.nn.silu(gate) * upper).astype(jnp.bfloat16)
    down = jnp.einsum("secf,efd->secd", hidden, w_down, preferred_element_type=jnp.float32)
    summed = lax.psum_scatter(down.astype(jnp.bfloat16), "tp", scatter_dimension=3, tiled=True)
    returned = lax.all_to_all(summed, "ep", split_axis=0, concat_axis=0, tiled=True)
    flat_back = returned.reshape(experts * cap, width // n_tp)
    picked = flat_back[place].astype(jnp.float32).reshape(ntok, top, width // n_tp)
    return jnp.sum(picked * route_w[:, :, None], axis=1).astype(jnp.bfloat16)


def body(
    mix_bgate,
    mix_cgate,
    mix_input,
    conv_taps,
    mix_out_w,
    moe_x,
    moe_gain,
    routes,
    route_w,
    w_gate,
    w_up,
    w_down,
):
    mixed = conv_mixer(mix_bgate, mix_cgate, mix_input, conv_taps, mix_out_w)
    routed = expert_layer(moe_x, moe_gain, routes, route_w, w_gate, w_up, w_down)
    return (mixed, routed)


def solution(mesh):
    in_specs = (
        P("ep", "tp"),
        P("ep", "tp"),
        P("ep", "tp"),
        P(None, "tp"),
        P("tp", None),
        P("ep", "tp"),
        P(),
        P("ep", None),
        P("ep", None),
        P("ep", None, "tp"),
        P("ep", None, "tp"),
        P("ep", "tp", None),
    )
    out_specs = (P(("ep", "tp"), None), P("ep", "tp"))
    return jax.shard_map(body, mesh=mesh, in_specs=in_specs, out_specs=out_specs, check_vma=False)
```

profile of v0, /device:TPU:0, one launch (start us, length us, event | category | flops | bytes accessed | tf_op | source)
XLA Modules:
  0.0 185.2 jit_solution(3375936974495529147)
XLA Ops:
  7.2 0.0 copy-start
  7.2 0.0 all-gather.3.cloned.1.call-start
  7.2 0.7 all-gather.3.cloned.1.call-update
  7.9 0.0 all-gather.5.cloned.1.call-start
  8.0 0.8 copy.20
  8.8 0.1 eq.29
  8.9 0.1 eq.25
  9.1 1.1 reduce-window.6
  10.2 0.2 slice_reduce_fusion
  10.5 0.7 broadcast_multiply_fusion
  11.2 0.1 copy.19
  11.3 0.1 mul.110
  11.5 0.1 fusion.43
  11.6 2.4 %scatter_custom_fusion = s32[768]{0:T(1024)S(1)} fusion(s32[512]{0:T(512)S(1)} %bitcast.108, s32[512]{0:T(512)S(1)} %add_select_fusion, s32[]{:T(128)} %constant.40.clone.1), kind=kCustom, calls=%fused_computation.57 | custom fusion | bytes 3076 | tf_op jit(solution)/shard_map/scatter | solution.py:57
  14.1 15.0 %all-gather.3.cloned.1.call-done = bf16[256,2048]{1,0:T(8,128)(2,1)} async-done(((bf16[256,512]{1,0:T(8,128)(2,1)}), bf16[256,2048]{1,0:T(8,128)(2,1)}) %all-gather.3.cloned.1.call-update) | async-done | bytes 1048592 | tf_op jit(solution)/shard_map/all_gather | solution.py:40
  29.0 1.5 fusion.18
  30.6 1.5 fusion.20
  32.1 0.1 concatenate.11
  32.2 4.3 %gather_fusion = bf16[768,2048]{1,0:T(8,128)(2,1)} fusion(bf16[257,2048]{1,0:T(8,128)(2,1)S(1)} %concatenate.11, s32[1024]{0:T(1024)S(1)} %pad_clamp_fusion.1), kind=kCustom, calls=%fused_computation | custom fusion | bytes 6294528 | tf_op jit(solution)/shard_map/gather | solution.py:60
  36.5 1.2 constant_dynamic-slice_fusion
  37.7 25.9 %all_to_all.10 = bf16[8,1,24,2048]{3,2,1,0:T(8,128)(2,1)} all-to-all(bf16[8,1,24,2048]{3,2,1,0:T(8,128)(2,1)S(1)} %constant_dynamic-slice_fusion), channel_id=1, replica_groups=mesh['ep'=8,'tp'=4] {'ep'}, dimensions={0} | all-to-all | bytes 1572864 | tf_op jit(solution)/shard_map/all_to_all | solution.py:63
  63.6 0.0 all-gather.5.cloned.1.call-update
  63.6 0.0 reduce-scatter.5.cloned.1.call-start
  63.7 26.7 %all-gather.5.cloned.1.call-done = bf16[8,1,96,2048]{3,2,0,1:T(8,128)(2,1)} async-done(((bf16[8,1,24,2048]{3,2,0,1:T(8,128)(2,1)}), bf16[8,1,96,2048]{3,2,0,1:T(8,128)(2,1)}) %all-gather.5.cloned.1.call-update) | async-done | bytes 3145744 | tf_op jit(solution)/shard_map/all_gather | solution.py:64
  90.4 8.0 %fusion.4 = f32[8,96,896]{2,1,0:T(8,128)} fusion(bf16[1,2048,896]{2,1,0:T(8,128)(2,1)} %param.21, bf16[8,1,96,2048]{3,2,0,1:T(8,128)(2,1)} %all-gather.5.cloned.1.call-done), kind=kOutput, calls=%fused_computation.7 | convolution fusion | flops 2818572288 | bytes 9568256 | tf_op jit(solution)/shard_map/secd,edf->secf/dot_general | solution.py:65
  98.4 12.1 %fusion.11 = bf16[8,1,96,2048]{3,2,0,1:T(8,128)(2,1)} fusion(bf16[1,896,2048]{2,1,0:T(8,128)(2,1)} %param.23, bf16[1,2048,896]{2,1,0:T(8,128)(2,1)} %param.22, bf16[8,1,96,2048]{3,2,0,1:T(8,128)(2,1)} %all-gather.5.cloned.1.call-done, f32[8,96,896]{2,1,0:T(8,128)} %fusion.4), kind=kOutput, calls=%fused_computation.12 | convolution fusion | flops 5642846208 | bytes 16384000 | tf_op jit(solution)/shard_map/secf,efd->secd/dot_general | solution.py:68
  110.5 0.0 copy-start.3
  110.5 0.0 reduce-scatter.5.cloned.1.call-update
  110.5 0.0 copy-start.5
  110.5 0.0 reduce-scatter.3.cloned.1.call-start
  110.6 0.8 copy-done.1
  111.4 0.1 copy-done.2
  111.5 3.4 %collective-permute-start = (bf16[2,2,256]{2,1,0:T(2,128)(2,1)S(1)}, bf16[2,2,256]{2,1,0:T(2,128)(2,1)S(1)}, u32[]{:S(2)}, u32[]{:S(2)}) collective-permute-start(bf16[2,2,256]{2,1,0:T(2,128)(2,1)S(1)} %pad_maximum_fusion), channel_id=1, source_target_pairs={{0,4},{4,8},{8,12},{12,16},{16,20},{20,24},{24,28},{1,5},{5,9},{9,... | collective-permute-start | bytes 6152 | tf_op jit(solution)/shard_map/ppermute | solution.py:10
  114.9 0.0 copy-done.4
  114.9 1.3 collective-permute-done
  116.2 0.1 convert_multiply_fusion.2
  116.2 0.0 copy-done
  116.2 0.0 copy-done.3
  116.2 1.5 convolution_convert_fusion
  117.7 0.0 reduce-scatter.3.cloned.1.call-update
  117.7 30.7 %reduce-scatter.5.cloned.1.call-done = bf16[8,1,96,512]{3,2,0,1:T(8,128)(2,1)} async-done(((bf16[8,1,96,2048]{3,2,0,1:T(8,128)(2,1)}), bf16[8,1,96,512]{3,2,0,1:T(8,128)(2,1)}) %reduce-scatter.5.cloned.1.call-update) | async-done | bytes 786448 | tf_op jit(solution)/shard_map/reduce_scatter | solution.py:69
  148.4 5.5 %all-to-all-start.1 = ((bf16[8,1,96,512]{3,2,1,0:T(8,128)(2,1)}), bf16[8,1,96,512]{3,2,1,0:T(8,128)(2,1)S(1)}, u32[]{:S(2)}, u32[]{:S(2)}) async-start(bf16[8,1,96,512]{3,2,1,0:T(8,128)(2,1)} %bitcast.107), calls=%async_computation.3 | async-start | bytes 1572864 | tf_op jit(solution)/shard_map/all_to_all | solution.py:70
  153.9 0.0 copy-done.5
  153.9 0.1 copy.25
  154.1 19.9 %all-to-all-done.1 = bf16[8,1,96,512]{3,2,1,0:T(8,128)(2,1)S(1)} async-done(((bf16[8,1,96,512]{3,2,1,0:T(8,128)(2,1)}), bf16[8,1,96,512]{3,2,1,0:T(8,128)(2,1)S(1)}, u32[]{:S(2)}, u32[]{:S(2)}) %all-to-all-start.1) | async-done | bytes 786464 | tf_op jit(solution)/shard_map/all_to_all | solution.py:70
  174.0 2.0 %gather_fusion.1 = bf16[512,512]{1,0:T(8,128)(2,1)S(1)} fusion(bf16[768,512]{1,0:T(8,128)(2,1)S(1)} %bitcast.104, s32[1024]{0:T(1024)S(1)} %pad_clamp_fusion), kind=kCustom, calls=%fused_computation.1 | custom fusion | bytes 1050624 | tf_op jit(solution)/shard_map/gather | solution.py:72
  176.0 0.7 reshape.98
  176.6 2.1 %multiply_reduce_fusion = bf16[256,512]{1,0:T(8,128)(2,1)} fusion(f32[256,2,512]{2,1,0:T(2,128)S(1)} %reshape.98, f32[256,2]{1,0:T(8,128)S(1)} %copy.25), kind=kLoop, calls=%fused_computation.27 | loop fusion | flops 393216 | bytes 1312768 | tf_op jit(solution)/shard_map/reduce_sum | solution.py:73
  (17 shorter events, 0.1 us)
Async XLA Ops:
  7.2 109.1 %copy-start = (bf16[256,2048]{1,0:T(8,128)(2,1)S(1)}, bf16[256,2048]{1,0:T(8,128)(2,1)}, u32[]{:S(2)}) copy-start(bf16[256,2048]{1,0:T(8,128)(2,1)} %param.16) | copy-start | bytes 3145732
  7.2 21.9 %all-gather.3.cloned.1.call-start = ((), (), s32[]{:S(2)}) async-start(), calls=%async_computation.5 | async-start | bytes 1310720 | tf_op jit(solution)/shard_map/all_gather | solution.py:40
  7.9 82.5 %all-gather.5.cloned.1.call-start = ((), (), s32[]{:S(2)}) async-start(), calls=%async_computation.6 | async-start | bytes 3932160 | tf_op jit(solution)/shard_map/all_gather | solution.py:64
  63.6 84.8 %reduce-scatter.5.cloned.1.call-start = ((), (), s32[]{:S(2)}) async-start(), calls=%async_computation.7 | async-start | bytes 3932160 | tf_op jit(solution)/shard_map/reduce_scatter | solution.py:69
  110.5 0.9 copy-start.1
  110.5 1.0 copy-start.2
  110.5 4.4 %copy-start.4 = (f32[3,256]{1,0:T(4,128)S(1)}, f32[3,256]{1,0:T(4,128)}, u32[]{:S(2)}) copy-start(f32[3,256]{1,0:T(4,128)} %param.15) | copy-start | bytes 9220
  110.5 5.7 %copy-start.3 = (bf16[256,256]{1,0:T(8,128)(2,1)S(1)}, bf16[256,256]{1,0:T(8,128)(2,1)}, u32[]{:S(2)}) copy-start(bf16[256,256]{1,0:T(8,128)(2,1)} %param.12) | copy-start | bytes 393220
  110.5 43.4 %copy-start.5 = (f32[256,2]{0,1:T(2,128)S(1)}, f32[256,2]{0,1:T(2,128)}, u32[]{:S(2)}) copy-start(f32[256,2]{0,1:T(2,128)} %param.20) | copy-start | bytes 6148
  110.5 68.1 %reduce-scatter.3.cloned.1.call-start = ((), (), s32[]{:S(2)}) async-start(), calls=%async_computation.4 | async-start | bytes 1310720 | tf_op jit(solution)/shard_map/reduce_scatter | solution.py:31
  111.5 4.7 %collective-permute-start = (bf16[2,2,256]{2,1,0:T(2,128)(2,1)S(1)}, bf16[2,2,256]{2,1,0:T(2,128)(2,1)S(1)}, u32[]{:S(2)}, u32[]{:S(2)}) collective-permute-start(bf16[2,2,256]{2,1,0:T(2,128)(2,1)S(1)} %pad_maximum_fusion), channel_id=1, source_target_pairs={{0,4},{4,8},{8,12},{12,16},{16,20},{20,24},{24,28},{1,5},{5,9},{9,... | collective-permute-start | bytes 6152 | tf_op jit(solution)/shard_map/ppermute | solution.py:10
  148.4 25.6 %all-to-all-start.1 = ((bf16[8,1,96,512]{3,2,1,0:T(8,128)(2,1)}), bf16[8,1,96,512]{3,2,1,0:T(8,128)(2,1)S(1)}, u32[]{:S(2)}, u32[]{:S(2)}) async-start(bf16[8,1,96,512]{3,2,1,0:T(8,128)(2,1)} %bitcast.107), calls=%async_computation.3 | async-start | bytes 1572864 | tf_op jit(solution)/shard_map/all_to_all | solution.py:70
Sparse Core Ops, SparseCore 0:
  9.5 19.4 all-gather.2
  63.7 26.6 all-gather.4
  110.7 37.7 reduce-scatter.4
  151.4 24.7 reduce-scatter.2
where the time goes:
time: 186 us; the launch traced here: 185 us
  waiting for transfers between devices  94.3 us (51%)
  blocking collectives  25.9 us (14%)
  matrix products  21.5 us (12%)
  between operations  14 us (8%)
  local copies, waits for them, and re-layouts  13.3 us (7%)
  starting transfers between devices  9.05 us (5%)
  other arithmetic  7.18 us (4%)
    reduce_scatter x1, waiting for transfers between devices, expert_layer(): lax.psum_scatter(down.astype(jnp.bfloat16), 'tp', scatter_dimension=3, ti...  30.7 us
    all_gather x1, waiting for transfers between devices, expert_layer(): arrived = lax.all_gather(landed, 'tp', axis=2, tiled=True)  26.7 us
    all_to_all x1, blocking collectives, expert_layer(): landed = lax.all_to_all(mine, 'ep', split_axis=0, concat_axis=0, tiled=True)  25.9 us
    all_to_all x1, waiting for transfers between devices, expert_layer(): lax.all_to_all(summed, 'ep', split_axis=0, concat_axis=0, tiled=True)  19.9 us
    all_gather x1, waiting for transfers between devices, expert_layer(): whole = lax.all_gather(moe_x, 'tp', axis=1, tiled=True)  15 us
    dot_general x1, matrix products, expert_layer(): jnp.einsum('secf,efd->secd', hidden, w_down, preferred_element_type=jnp.f...  12.1 us
    dot_general x1, matrix products, expert_layer(): jnp.einsum('secd,edf->secf', arrived, w_gate, preferred_element_type=jnp....  8 us
    all_to_all x1, starting transfers between devices, expert_layer(): lax.all_to_all(summed, 'ep', split_axis=0, concat_axis=0, tiled=True)  5.52 us
  transfers between devices with their start and end apart: 6, of which 5 were waited for; matrix products, arithmetic and copies ran while one was open for 7% of the time, Pallas kernels for 0%

commit v1 on v0

v1 whole, which is shorter than its diff:
```python
import functools

import jax
import jax.numpy as jnp
from jax import lax
from jax.experimental import pallas as pl
from jax.experimental.pallas import tpu as pltpu
from jax.sharding import PartitionSpec as P


F32 = jnp.float32
BF16 = jnp.bfloat16
VMEM = pl.BlockSpec(memory_space=pltpu.VMEM)
SMEM = pl.BlockSpec(memory_space=pltpu.SMEM)
HBM = pl.BlockSpec(memory_space=pltpu.HBM)


def swap(block, bit):
    n = lax.axis_size("tp")
    return lax.ppermute(block, "tp", [(i, i ^ bit) for i in range(n)])


def pair_swap(block, b):
    n_ep, n_tp = lax.axis_size("ep"), lax.axis_size("tp")
    route = [
        (i * n_tp + q, (i ^ (b + (q & 1))) * n_tp + q)
        for i in range(n_ep)
        for q in range(n_tp)
    ]
    return lax.ppermute(block, ("ep", "tp"), route)


def shifted(block, distance):
    devices = range(lax.axis_size("ep"))
    route = [(i - distance, i) for i in devices if i - distance in devices]
    return lax.ppermute(block, "ep", route)


def bits_of(n):
    return [1 << k for k in range(n.bit_length() - 1)]


def total(terms):
    out = terms[0].astype(F32)
    for term in terms[1:]:
        out = out + term.astype(F32)
    return out


def spread_far(own):
    pieces = {0: own}
    for bit in reversed(bits_of(lax.axis_size("tp") // 2)):
        for r in list(pieces):
            pieces[r ^ bit] = swap(pieces[r], 2 * bit)
    return [pieces[r] for r in range(len(pieces))]


def reduce_far(kept, sent):
    live = {}
    for r in reversed(range(len(kept))):
        live[r] = [kept[r], swap(sent[r], 1)]
    for bit in reversed(bits_of(len(kept))):
        for r in [r for r in sorted(live) if r & bit]:
            value = total(live.pop(r)).astype(BF16)
            live[r ^ bit].append(swap(value, 2 * bit))
    return total(live[0]).astype(BF16)


def aligned(start, size):
    return pl.ds(pl.multiple_of(start * size, size), size)


def in_hbm(*arrays):
    return [pltpu.with_memory_space_constraint(a, pltpu.HBM) for a in arrays]


def fetch(pairs, sem):
    copies = [
        pltpu.make_async_copy(src, dst, sem.at[k]) for k, (src, dst) in enumerate(pairs)
    ]
    for copy in copies:
        copy.start()
    return copies


def mixer_kernel(n_tp, me_ref, halo_ref, b_hbm, c_hbm, x_hbm, taps_hbm, w_hbm, *refs):
    outs, refs = refs[:n_tp], refs[n_tp:]
    b_ref, c_ref, x_ref, taps_ref, w_ref, gated_ref, sem = refs
    copies = fetch(
        [(c_hbm, c_ref), (x_hbm, x_ref), (taps_hbm, taps_ref), (b_hbm, b_ref), (w_hbm, w_ref)],
        sem,
    )
    for copy in copies[:-1]:
        copy.wait()
    length = x_ref.shape[0]
    reach = taps_ref.shape[0] - 1
    prod = c_ref[...].astype(F32) * x_ref[...].astype(F32)
    before = halo_ref[0].astype(F32) * halo_ref[1].astype(F32)
    row = lax.broadcasted_iota(jnp.int32, prod.shape, 0)
    conv = taps_ref[reach : reach + 1, :] * prod
    for back in range(1, reach + 1):
        moved = pltpu.roll(prod, back, 0)
        for r in range(back):
            k = reach - back + r
            moved = jnp.where(row == r, before[k : k + 1, :], moved)
        conv = conv + taps_ref[reach - back : reach - back + 1, :] * moved
    gated_ref[...] = (b_ref[...].astype(F32) * conv).astype(BF16)
    part = length // n_tp
    copies[-1].wait()
    for r in range(n_tp):
        rows = gated_ref[aligned(me_ref[2] ^ r, part), :]
        outs[r][...] = jnp.dot(rows, w_ref[...], preferred_element_type=F32).astype(BF16)


def conv_mixer(at, mix_bgate, mix_cgate, mix_input, conv_taps, mix_out_w):
    n_tp = lax.axis_size("tp")
    length, chans = mix_input.shape
    width = mix_out_w.shape[1]
    reach = conv_taps.shape[0] - 1
    tail = jnp.stack([mix_cgate[length - reach :], mix_input[length - reach :]])
    halo = shifted(tail, 1)
    out = jax.ShapeDtypeStruct((length // n_tp, width), BF16)
    pieces = pl.pallas_call(
        functools.partial(mixer_kernel, n_tp),
        out_shape=[out] * n_tp,
        in_specs=[SMEM, VMEM] + [HBM] * 5,
        out_specs=[VMEM] * n_tp,
        scratch_shapes=[
            pltpu.VMEM((length, chans), BF16),
            pltpu.VMEM((length, chans), BF16),
            pltpu.VMEM((length, chans), BF16),
            pltpu.VMEM(conv_taps.shape, F32),
            pltpu.VMEM(mix_out_w.shape, BF16),
            pltpu.VMEM((length, chans), BF16),
            pltpu.SemaphoreType.DMA((5,)),
        ],
        compiler_params=pltpu.CompilerParams(vmem_limit_bytes=16 << 20),
        cost_estimate=pl.CostEstimate(
            flops=2 * length * chans * width, bytes_accessed=3 << 20, transcendentals=0
        ),
        name="mixer",
    )(at, halo, *in_hbm(mix_bgate, mix_cgate, mix_input, conv_taps, mix_out_w))
    near = range(0, n_tp, 2)
    return reduce_far([pieces[r] for r in near], [pieces[r + 1] for r in near])


def dispatch_kernel(n_ep, cap, at_ref, own_hbm, other_ref, routes_hbm, weight_hbm, *refs):
    blocks, refs = refs[: n_ep // 2], refs[n_ep // 2 :]
    slot_out, weight_out, both, routes_ref, weight_ref, sem = refs
    core = at_ref[1]
    part = other_ref.shape[1]
    copies = fetch(
        [
            (routes_hbm, routes_ref),
            (weight_hbm, weight_ref),
            (own_hbm, both.at[:, aligned(core, part)]),
        ],
        sem,
    )
    both[:, aligned(1 - core, part)] = other_ref[...]
    copies[0].wait()
    copies[1].wait()
    rel = routes_ref[...] ^ at_ref[0]
    top, ntok = rel.shape
    expert = 2 * lax.broadcasted_iota(jnp.int32, (n_ep // 2, ntok), 0)
    named = rel[0:1, :] == expert
    weight = jnp.where(named, weight_ref[0:1, :], 0.0)
    for k in range(1, top):
        here = rel[k : k + 1, :] == expert
        weight = weight + jnp.where(here, weight_ref[k : k + 1, :], 0.0)
        named = named | here
    before = lax.broadcasted_iota(jnp.int32, (ntok, ntok), 0) < lax.broadcasted_iota(
        jnp.int32, (ntok, ntok), 1
    )
    slot = jnp.dot(
        named.astype(F32).astype(BF16),
        before.astype(F32).astype(BF16),
        preferred_element_type=F32,
    )
    slot = jnp.where(named, slot, -1.0)
    slot_out[...] = slot
    weight_out[...] = weight
    rows = lax.broadcasted_iota(jnp.int32, (cap, ntok), 0).astype(F32)
    copies[2].wait()
    for j in range(n_ep // 2):
        pick = (rows == slot[j : j + 1, :]).astype(F32).astype(BF16)
        blocks[j][...] = jnp.dot(pick, both[...], preferred_element_type=F32).astype(BF16)


def expert_kernel(n_far, me_ref, gain_ref, wg_ref, wu_ref, wd_ref, *refs):
    own, refs = refs[:n_far], refs[n_far:]
    other, refs = refs[:n_far], refs[n_far:]
    kept, refs = refs[:n_far], refs[n_far:]
    sent, (rows_ref,) = refs[:n_far], refs[n_far:]
    half, part = own[0].shape
    me = me_ref[3]
    scales = []
    for refs in (own, other):
        square = None
        for ref in refs:
            wide = ref[...].astype(F32)
            term = jnp.sum(wide * wide, axis=1, keepdims=True)
            square = term if square is None else square + term
        scales.append(lax.rsqrt(square / (part * n_far) + 1e-06))
    gate = up = None
    for r in range(n_far):
        at = aligned(me ^ r, part)
        for k, ref in enumerate((own[r], other[r])):
            normed = ref[...].astype(F32) * scales[k] * gain_ref[:, at]
            rows_ref[r, k * half : (k + 1) * half, :] = normed.astype(BF16)
        g = jnp.dot(rows_ref[r], wg_ref[0, at, :], preferred_element_type=F32)
        u = jnp.dot(rows_ref[r], wu_ref[0, at, :], preferred_element_type=F32)
        gate = g if gate is None else gate + g
        up = u if up is None else up + u
    hidden = (gate / (1.0 + jnp.exp(-gate)) * up).astype(BF16)
    for r in reversed(range(n_far)):
        at = aligned(me ^ r, part)
        out = jnp.dot(hidden, wd_ref[0, :, at], preferred_element_type=F32).astype(BF16)
        kept[r][...] = out[:half]
        sent[r][...] = out[half:]


def combine_kernel(rows_of, last, at_ref, slot_ref, weight_ref, *refs):
    n = len(rows_of)
    blocks, refs = refs[:n], refs[n:]
    acc = None
    if last:
        before_ref, sent_ref, kept_ref, sum_ref = refs
        acc = before_ref[...]
    else:
        (sum_ref,) = refs
    ntok = sum_ref.shape[0]
    contract = (((0,), (0,)), ((), ()))
    for ref, j in zip(blocks, rows_of):
        rows = lax.broadcasted_iota(jnp.int32, (ref.shape[0], ntok), 0).astype(F32)
        spread = jnp.where(rows == slot_ref[j : j + 1, :], weight_ref[j : j + 1, :], 0.0)
        high = spread.astype(BF16)
        low = (spread - high.astype(F32)).astype(BF16)
        block = ref[...]
        term = lax.dot_general(high, block, contract, preferred_element_type=F32)
        term = term + lax.dot_general(low, block, contract, preferred_element_type=F32)
        acc = term if acc is None else acc + term
    sum_ref[...] = acc
    if last:
        part = kept_ref.shape[1]
        kept_ref[...] = sum_ref[:, aligned(at_ref[1], part)]
        sent_ref[...] = sum_ref[:, aligned(1 - at_ref[1], part)].astype(BF16)


def expert_layer(at, moe_x, moe_gain, routes, route_w, w_gate, w_up, w_down):
    ntok, part = moe_x.shape
    top = routes.shape[1]
    n_ep, n_tp = lax.axis_size("ep"), lax.axis_size("tp")
    n_far = n_tp // 2
    assert w_gate.shape[0] == 1
    cap = 4 * ((3 * ntok * top + 8 * n_ep - 1) // (8 * n_ep))
    gain = moe_gain.reshape(1, -1)
    wide = 2 * part
    n_ops = n_ep // 2
    n_groups = min(4, n_ops)
    per_group = n_ops // n_groups

    other_x = swap(moe_x, 1)
    block = jax.ShapeDtypeStruct((cap, wide), BF16)
    table = jax.ShapeDtypeStruct((n_ops, ntok), F32)
    *sent, slots, weights = pl.pallas_call(
        functools.partial(dispatch_kernel, n_ep, cap),
        out_shape=[block] * n_ops + [table] * 2,
        in_specs=[SMEM, HBM, VMEM, HBM, HBM],
        out_specs=[VMEM] * (n_ops + 2),
        scratch_shapes=[
            pltpu.VMEM((ntok, wide), BF16),
            pltpu.VMEM((top, ntok), jnp.int32),
            pltpu.VMEM((top, ntok), F32),
            pltpu.SemaphoreType.DMA((3,)),
        ],
        compiler_params=pltpu.CompilerParams(vmem_limit_bytes=16 << 20),
        cost_estimate=pl.CostEstimate(
            flops=1 << 36, bytes_accessed=1 << 20, transcendentals=0
        ),
        name="dispatch",
    )(at, *in_hbm(moe_x), other_x, *in_hbm(routes.T, route_w.T))
    stack = [w_gate, w_up, w_down]
    back = {}
    for g in ORDER[n_groups]:
        ops = range(g * per_group, (g + 1) * per_group)
        landed = [pair_swap(sent[j], 2 * j) for j in ops]
        own = landed[0] if per_group == 1 else jnp.concatenate(landed, 0)
        own = spread_far(own)
        other = [swap(own[r], 1) for r in range(n_far)]
        rows = per_group * cap
        out = jax.ShapeDtypeStruct((rows, wide), BF16)
        results = pl.pallas_call(
            functools.partial(expert_kernel, n_far),
            out_shape=[out] * (2 * n_far),
            in_specs=[SMEM] + [VMEM] * (4 + 2 * n_far),
            out_specs=[VMEM] * (2 * n_far),
            scratch_shapes=[pltpu.VMEM((n_far, 2 * rows, wide), BF16)],
            compiler_params=pltpu.CompilerParams(vmem_limit_bytes=24 << 20),
            cost_estimate=pl.CostEstimate(
                flops=12 * rows * wide * n_far * w_gate.shape[2],
                bytes_accessed=8 * rows * wide * n_far,
                transcendentals=2 * rows * w_gate.shape[2],
            ),
            name="experts",
        )(at, gain, *stack, *own, *other)
        done = reduce_far(results[:n_far], results[n_far:])
        for k, j in enumerate(ops):
            back[j] = pair_swap(done[k * cap : (k + 1) * cap], 2 * j)

    def combine(rows_of, before):
        kept = jax.ShapeDtypeStruct((ntok, part), F32)
        crossing = jax.ShapeDtypeStruct((ntok, part), BF16)
        acc = jax.ShapeDtypeStruct((ntok, wide), F32)
        outs = [crossing, kept] if before else [acc]
        return pl.pallas_call(
            functools.partial(combine_kernel, rows_of, bool(before)),
            out_shape=outs,
            in_specs=[SMEM] + [VMEM] * (2 + len(rows_of) + len(before)),
            out_specs=[VMEM] * len(outs),
            scratch_shapes=[pltpu.VMEM(acc.shape, F32)] if before else [],
            compiler_params=pltpu.CompilerParams(vmem_limit_bytes=16 << 20),
            cost_estimate=pl.CostEstimate(
                flops=4 * len(rows_of) * cap * ntok * wide,
                bytes_accessed=1 << 20,
                transcendentals=0,
            ),
            name="combine",
        )(at, slots, weights, *[back[j] for j in rows_of], *before)

    final = ORDER[n_groups][-1]
    late = [j for j in range(n_ops) if j // per_group == final]
    early = [j for j in range(n_ops) if j not in late]
    acc = combine(early, [])
    crossing, kept = combine(late, acc)
    crossed = swap(crossing, 1)
    return (kept + crossed.astype(F32)).astype(BF16)


ORDER = {1: [0], 2: [1, 0], 4: [2, 0, 3, 1]}


def body(
    mix_bgate,
    mix_cgate,
    mix_input,
    conv_taps,
    mix_out_w,
    moe_x,
    moe_gain,
    routes,
    route_w,
    w_gate,
    w_up,
    w_down,
):
    ep = lax.axis_index("ep").astype(jnp.int32)
    tp = lax.axis_index("tp").astype(jnp.int32)
    core = tp & 1
    at = jnp.stack([ep ^ core, core, tp, tp >> 1])
    mixed = conv_mixer(at, mix_bgate, mix_cgate, mix_input, conv_taps, mix_out_w)
    routed = expert_layer(at, moe_x, moe_gain, routes, route_w, w_gate, w_up, w_down)
    return (mixed, routed)


def solution(mesh):
    in_specs = (
        P("ep", "tp"),
        P("ep", "tp"),
        P("ep", "tp"),
        P(None, "tp"),
        P("tp", None),
        P("ep", "tp"),
        P(),
        P("ep", None),
        P("ep", None),
        P("ep", None, "tp"),
        P("ep", None, "tp"),
        P("ep", "tp", None),
    )
    out_specs = (P(("ep", "tp"), None), P("ep", "tp"))
    return jax.shard_map(body, mesh=mesh, in_specs=in_specs, out_specs=out_specs, check_vma=False)
```

time: 186 us -> 111 us (0.60)
  waiting for transfers between devices: 94.3 us -> 48.8 us
  starting transfers between devices: 9.05 us -> 36.3 us
  blocking collectives: 25.9 us -> 0 us
  matrix products: 21.5 us -> 0 us
  Pallas kernels: 0 us -> 21.4 us
  between operations: 14 us -> 0.96 us
  local copies, waits for them, and re-layouts: 13.3 us -> 0.72 us
  other arithmetic: 7.18 us -> 2.25 us
    ppermute x1 -> x38, waiting for transfers between devices: 1.27 us -> 48.8 us  [the longest x29 27.9 us: swap(): return lax.ppermute(block, 'tp', [(i, i ^ bit) for i in range(n)])]
    all_gather x2 -> x0, waiting for transfers between devices: 41.7 us -> none  [the longest x1 26.7 us: expert_layer(): arrived = lax.all_gather(landed, 'tp', axis=2, tiled=True)]
    ppermute x1 -> x38, starting transfers between devices: 3.38 us -> 36.3 us  [the longest x29 16.5 us: swap(): return lax.ppermute(block, 'tp', [(i, i ^ bit) for i in range(n)])]
    reduce_scatter x2 -> x0, waiting for transfers between devices: 30.7 us -> none  [the longest x1 30.7 us: expert_layer(): lax.psum_scatter(down.astype(jnp.bfloat16), 'tp', scatter_dimension=3, ti...]
    all_to_all x1 -> x0, blocking collectives: 25.9 us -> none  [expert_layer(): landed = lax.all_to_all(mine, 'ep', split_axis=0, concat_axis=0, tiled=True)]
    dot_general x3 -> x0, matrix products: 21.5 us -> none  [the longest x1 12.1 us: expert_layer(): jnp.einsum('secf,efd->secd', hidden, w_down, preferred_element_type=jnp.f...]
    pallas_call x0 -> x8, Pallas kernels: none -> 21.4 us  [the longest x4 13.6 us: expert_layer(): pl.pallas_call(functools.partial(expert_kernel, n_far), out_shape=[out] *...]
    all_to_all x1 -> x0, waiting for transfers between devices: 19.9 us -> none  [expert_layer(): lax.all_to_all(summed, 'ep', split_axis=0, concat_axis=0, tiled=True)]
  transfers between devices with their start and end apart: 6 -> 38, of which waited for: 5 -> 15; matrix products, arithmetic and copies ran while one was open for 7% -> 2% of each run, Pallas kernels for 0% -> 17%
where the time goes in v1:
time: 111 us
  waiting for transfers between devices  48.8 us (44%)
  starting transfers between devices  36.3 us (33%)
  Pallas kernels  21.4 us (19%)
  other arithmetic  2.25 us (2%)
    ppermute x29, waiting for transfers between devices, swap(): return lax.ppermute(block, 'tp', [(i, i ^ bit) for i in range(n)])  27.9 us
    ppermute x8, waiting for transfers between devices, pair_swap(): return lax.ppermute(block, ('ep', 'tp'), route)  19.6 us
    ppermute x29, starting transfers between devices, swap(): return lax.ppermute(block, 'tp', [(i, i ^ bit) for i in range(n)])  16.5 us
    ppermute x8, starting transfers between devices, pair_swap(): return lax.ppermute(block, ('ep', 'tp'), route)  16.4 us
    pallas_call x4, Pallas kernels, expert_layer(): pl.pallas_call(functools.partial(expert_kernel, n_far), out_shape=[out] *...  13.6 us
    ppermute x1, starting transfers between devices, shifted(): return lax.ppermute(block, 'ep', route)  3.38 us
    pallas_call x1, Pallas kernels, conv_mixer(): pl.pallas_call(functools.partial(mixer_kernel, n_tp), out_shape=[out] * n...  2.89 us
    pallas_call x2, Pallas kernels, combine(): pl.pallas_call(functools.partial(combine_kernel, rows_of, bool(before)),...  2.6 us
  transfers between devices with their start and end apart: 38, of which 15 were waited for; matrix products, arithmetic and copies ran while one was open for 2% of the time, Pallas kernels for 17%

profile of v1, /device:TPU:0, one launch (start us, length us, event | category | flops | bytes accessed | tf_op | source)
XLA Modules:
  0.0 110.5 jit_solution(16976384000734999117)
XLA Ops:
  0.6 0.6 collective-permute-start.4
  1.3 0.7 slice_bitcast_fusion
  2.0 0.6 collective-permute-done.4.other_ref
  2.6 2.3 %dispatch.1 = (bf16[96,1024]{1,0:T(8,128)(2,1)S(1)}, bf16[96,1024]{1,0:T(8,128)(2,1)S(1)}, bf16[96,1024]{1,0:T(8,128)(2,1)S(1)}, bf16[96,1024]{1,0:T(8,128)(2,1)...) custom-call(s32[4]{0:T(128)S(1)} %pad_add_fusion.me_ref.at_ref, bf16[256,512]{1,0:T(8,128)(2,1)} %own_hbm.1, ...), custom_call_target="tpu_custom_call" | custom-call | flops 68719476736 | bytes 1048576 | tf_op jit(solution)/shard_map/dispatch/pallas_call | solution.py:266
  4.9 3.0 %collective-permute-start.5 = (bf16[96,1024]{1,0:T(8,128)(2,1)S(1)}, bf16[96,1024]{1,0:T(8,128)(2,1)S(1)}, u32[]{:S(2)}, u32[]{:S(2)}) collective-permute-start(bf16[96,1024]{1,0:T(8,128)(2,1)S(1)} %get-tuple-element.36), channel_id=1, source_target_pairs={{0,8},{1,13},{2,10},{3,15},{4,12},{5,9},{6,14},{7,11},{8,0},{9,5},... | collective-permute-start | bytes 589832 | tf_op jit(solution)/shard_map/ppermute | solution.py:30
  7.9 3.4 %collective-permute-start = (bf16[2,2,256]{2,1,0:T(2,128)(2,1)S(1)}, bf16[2,2,256]{2,1,0:T(2,128)(2,1)S(1)}, u32[]{:S(2)}, u32[]{:S(2)}) collective-permute-start(bf16[2,2,256]{2,1,0:T(2,128)(2,1)S(1)} %pad_maximum_fusion), channel_id=1, source_target_pairs={{0,4},{4,8},{8,12},{12,16},{16,20},{20,24},{24,28},{1,5},{5,9},{9,... | collective-permute-start | bytes 6152 | tf_op jit(solution)/shard_map/ppermute | solution.py:36
  11.3 1.3 %collective-permute-done.halo_ref = bf16[2,2,256]{2,1,0:T(2,128)(2,1)S(1)} collective-permute-done((bf16[2,2,256]{2,1,0:T(2,128)(2,1)S(1)}, bf16[2,2,256]{2,1,0:T(2,128)(2,1)S(1)}, u32[]{:S(2)}, u32[]{:S(2)}) %collective-permute-start) | collective-permute-done | bytes 2080 | tf_op jit(solution)/shard_map/ppermute | solution.py:36
  12.6 2.9 %mixer.1 = (bf16[64,2048]{1,0:T(8,128)(2,1)S(1)}, bf16[64,2048]{1,0:T(8,128)(2,1)S(1)}, bf16[64,2048]{1,0:T(8,128)(2,1)S(1)}, bf16[64,2048]{1,0:T(8,128)(2,1)S(1)}) custom-call(s32[4]{0:T(128)S(1)} %pad_add_fusion.me_ref.at_ref, bf16[2,2,256]{2,1,0:T(2,128)(2,1)S(1)} %collective-permute-done.halo_ref, bf16[256,256]{1,0:T(8,128)(2,1)} %b_hbm.1, ...), custom_call_target="tpu_custom_call" | custom-call | flops 268435456 | bytes 3145728 | tf_op jit(solution)/shard_map/mixer/pallas_call | solution.py:123
  15.6 0.7 collective-permute-start.13
  16.3 1.6 %collective-permute-start.6 = (bf16[96,1024]{1,0:T(8,128)(2,1)S(1)}, bf16[96,1024]{1,0:T(8,128)(2,1)S(1)}, u32[]{:S(2)}, u32[]{:S(2)}) collective-permute-start(bf16[96,1024]{1,0:T(8,128)(2,1)S(1)} %collective-permute-done.5.refs_0_), channel_id=1, source_target_pairs={{0,2},{1,3},{2,0},{3,1},{4,6},{5,7},{6,4},{7,5},{8,10},{9,11},{10,... | collective-permute-start | bytes 589832 | tf_op jit(solution)/shard_map/ppermute | solution.py:20
  17.8 3.5 %collective-permute-start.1 = (bf16[64,2048]{1,0:T(8,128)(2,1)S(1)}, bf16[64,2048]{1,0:T(8,128)(2,1)S(1)}, u32[]{:S(2)}, u32[]{:S(2)}) collective-permute-start(bf16[64,2048]{1,0:T(8,128)(2,1)S(1)} %get-tuple-element.31), channel_id=1, source_target_pairs={{0,1},{1,0},{2,3},{3,2},{4,5},{5,4},{6,7},{7,6},{8,9},{9,8},{10,11... | collective-permute-start | bytes 786440 | tf_op jit(solution)/shard_map/ppermute | solution.py:20
  21.3 2.6 %collective-permute-start.21 = (bf16[96,1024]{1,0:T(8,128)(2,1)S(1)}, bf16[96,1024]{1,0:T(8,128)(2,1)S(1)}, u32[]{:S(2)}, u32[]{:S(2)}) collective-permute-start(bf16[96,1024]{1,0:T(8,128)(2,1)S(1)} %get-tuple-element.46), channel_id=1, source_target_pairs={{0,16},{1,21},{2,18},{3,23},{4,20},{5,17},{6,22},{7,19},{8,24},{9,... | collective-permute-start | bytes 589832 | tf_op jit(solution)/shard_map/ppermute | solution.py:30
  23.9 0.6 collective-permute-start.7
  24.5 0.5 collective-permute-start.14
  25.1 8.1 %collective-permute-done.21.refs_0_ = bf16[96,1024]{1,0:T(8,128)(2,1)S(1)} collective-permute-done((bf16[96,1024]{1,0:T(8,128)(2,1)S(1)}, bf16[96,1024]{1,0:T(8,128)(2,1)S(1)}, u32[]{:S(2)}, u32[]{:S(2)}) %collective-permute-start.21) | collective-permute-done | bytes 196640 | tf_op jit(solution)/shard_map/ppermute | solution.py:30
  33.2 4.0 %collective-permute-start.29 = (bf16[96,1024]{1,0:T(8,128)(2,1)S(1)}, bf16[96,1024]{1,0:T(8,128)(2,1)S(1)}, u32[]{:S(2)}, u32[]{:S(2)}) collective-permute-start(bf16[96,1024]{1,0:T(8,128)(2,1)S(1)} %get-tuple-element.51), channel_id=1, source_target_pairs={{0,24},{1,29},{2,26},{3,31},{4,28},{5,25},{6,30},{7,27},{8,16},{9,... | collective-permute-start | bytes 589832 | tf_op jit(solution)/shard_map/ppermute | solution.py:30
  37.2 0.6 collective-permute-start.15
  37.8 0.5 collective-permute-start.22
  38.4 3.4 %experts.4 = (bf16[96,1024]{1,0:T(8,128)(2,1)S(1)}, bf16[96,1024]{1,0:T(8,128)(2,1)S(1)}, bf16[96,1024]{1,0:T(8,128)(2,1)S(1)}, bf16[96,1024]{1,0:T(8,128)(2,1)S(1)}) custom-call(s32[4]{0:T(128)S(1)} %pad_add_fusion.me_ref.at_ref, f32[1,2048]{1,0:T(1,128)S(1)} %bitcast.11, bf16[1,2048,896]{2,1,0:T(8,128)(2,1)S(1)} %copy-done, ...), custom_call_target="tpu_custom_call" | custom-call | flops 2113929216 | bytes 1572864 | tf_op jit(solution)/shard_map/experts/pallas_call | solution.py:293
  41.8 0.7 collective-permute-done.29.refs_0_
  42.5 0.9 collective-permute-start.3
  43.6 1.1 %collective-permute-done.22.refs_1_ = bf16[96,1024]{1,0:T(8,128)(2,1)S(1)} collective-permute-done((bf16[96,1024]{1,0:T(8,128)(2,1)S(1)}, bf16[96,1024]{1,0:T(8,128)(2,1)S(1)}, u32[]{:S(2)}, u32[]{:S(2)}) %collective-permute-start.22) | collective-permute-done | bytes 196640 | tf_op jit(solution)/shard_map/ppermute | solution.py:20
  45.2 3.4 %experts.5 = (bf16[96,1024]{1,0:T(8,128)(2,1)S(1)}, bf16[96,1024]{1,0:T(8,128)(2,1)S(1)}, bf16[96,1024]{1,0:T(8,128)(2,1)S(1)}, bf16[96,1024]{1,0:T(8,128)(2,1)S(1)}) custom-call(s32[4]{0:T(128)S(1)} %pad_add_fusion.me_ref.at_ref, f32[1,2048]{1,0:T(1,128)S(1)} %bitcast.12, bf16[1,2048,896]{2,1,0:T(8,128)(2,1)S(1)} %copy-done, ...), custom_call_target="tpu_custom_call" | custom-call | flops 2113929216 | bytes 1572864 | tf_op jit(solution)/shard_map/experts/pallas_call | solution.py:293
  48.6 0.6 collective-permute-start.31
  49.2 5.8 %collective-permute-done.30.refs_1_ = bf16[96,1024]{1,0:T(8,128)(2,1)S(1)} collective-permute-done((bf16[96,1024]{1,0:T(8,128)(2,1)S(1)}, bf16[96,1024]{1,0:T(8,128)(2,1)S(1)}, u32[]{:S(2)}, u32[]{:S(2)}) %collective-permute-start.30) | collective-permute-done | bytes 196640 | tf_op jit(solution)/shard_map/ppermute | solution.py:20
  55.0 0.5 collective-permute-start.9
  55.5 3.4 %experts.6 = (bf16[96,1024]{1,0:T(8,128)(2,1)S(1)}, bf16[96,1024]{1,0:T(8,128)(2,1)S(1)}, bf16[96,1024]{1,0:T(8,128)(2,1)S(1)}, bf16[96,1024]{1,0:T(8,128)(2,1)S(1)}) custom-call(s32[4]{0:T(128)S(1)} %pad_add_fusion.me_ref.at_ref, f32[1,2048]{1,0:T(1,128)S(1)} %bitcast.13, bf16[1,2048,896]{2,1,0:T(8,128)(2,1)S(1)} %copy-done, ...), custom_call_target="tpu_custom_call" | custom-call | flops 2113929216 | bytes 1572864 | tf_op jit(solution)/shard_map/experts/pallas_call | solution.py:293
  59.5 3.4 %experts.7 = (bf16[96,1024]{1,0:T(8,128)(2,1)S(1)}, bf16[96,1024]{1,0:T(8,128)(2,1)S(1)}, bf16[96,1024]{1,0:T(8,128)(2,1)S(1)}, bf16[96,1024]{1,0:T(8,128)(2,1)S(1)}) custom-call(s32[4]{0:T(128)S(1)} %pad_add_fusion.me_ref.at_ref, f32[1,2048]{1,0:T(1,128)S(1)} %bitcast.14, bf16[1,2048,896]{2,1,0:T(8,128)(2,1)S(1)} %copy-done, ...), custom_call_target="tpu_custom_call" | custom-call | flops 2113929216 | bytes 1572864 | tf_op jit(solution)/shard_map/experts/pallas_call | solution.py:293
  63.2 1.3 %collective-permute-done.18 = bf16[96,1024]{1,0:T(8,128)(2,1)S(1)} collective-permute-done((bf16[96,1024]{1,0:T(8,128)(2,1)S(1)}, bf16[96,1024]{1,0:T(8,128)(2,1)S(1)}, u32[]{:S(2)}, u32[]{:S(2)}) %collective-permute-start.18) | collective-permute-done | bytes 196640 | tf_op jit(solution)/shard_map/ppermute | solution.py:20
  64.7 1.2 %collective-permute-done.26 = bf16[96,1024]{1,0:T(8,128)(2,1)S(1)} collective-permute-done((bf16[96,1024]{1,0:T(8,128)(2,1)S(1)}, bf16[96,1024]{1,0:T(8,128)(2,1)S(1)}, u32[]{:S(2)}, u32[]{:S(2)}) %collective-permute-start.26) | collective-permute-done | bytes 196640 | tf_op jit(solution)/shard_map/ppermute | solution.py:20
  66.1 1.2 %collective-permute-done.34 = bf16[96,1024]{1,0:T(8,128)(2,1)S(1)} collective-permute-done((bf16[96,1024]{1,0:T(8,128)(2,1)S(1)}, bf16[96,1024]{1,0:T(8,128)(2,1)S(1)}, u32[]{:S(2)}, u32[]{:S(2)}) %collective-permute-start.34) | collective-permute-done | bytes 196640 | tf_op jit(solution)/shard_map/ppermute | solution.py:20
  67.3 1.3 %collective-permute-start.19 = (bf16[96,1024]{1,0:T(8,128)(2,1)S(1)}, bf16[96,1024]{1,0:T(8,128)(2,1)S(1)}, u32[]{:S(2)}, u32[]{:S(2)}) collective-permute-start(bf16[96,1024]{1,0:T(8,128)(2,1)S(1)} %add_convert_fusion.8), channel_id=1, source_target_pairs={{0,2},{1,3},{2,0},{3,1},{4,6},{5,7},{6,4},{7,5},{8,10},{9,11},{10,... | collective-permute-start | bytes 589832 | tf_op jit(solution)/shard_map/ppermute | solution.py:20
  68.8 5.5 %collective-permute-done.19 = bf16[96,1024]{1,0:T(8,128)(2,1)S(1)} collective-permute-done((bf16[96,1024]{1,0:T(8,128)(2,1)S(1)}, bf16[96,1024]{1,0:T(8,128)(2,1)S(1)}, u32[]{:S(2)}, u32[]{:S(2)}) %collective-permute-start.19) | collective-permute-done | bytes 196640 | tf_op jit(solution)/shard_map/ppermute | solution.py:20
  74.3 1.3 %collective-permute-start.27 = (bf16[96,1024]{1,0:T(8,128)(2,1)S(1)}, bf16[96,1024]{1,0:T(8,128)(2,1)S(1)}, u32[]{:S(2)}, u32[]{:S(2)}) collective-permute-start(bf16[96,1024]{1,0:T(8,128)(2,1)S(1)} %add_convert_fusion.6), channel_id=1, source_target_pairs={{0,2},{1,3},{2,0},{3,1},{4,6},{5,7},{6,4},{7,5},{8,10},{9,11},{10,... | collective-permute-start | bytes 589832 | tf_op jit(solution)/shard_map/ppermute | solution.py:20
  75.8 4.6 %collective-permute-done.27 = bf16[96,1024]{1,0:T(8,128)(2,1)S(1)} collective-permute-done((bf16[96,1024]{1,0:T(8,128)(2,1)S(1)}, bf16[96,1024]{1,0:T(8,128)(2,1)S(1)}, u32[]{:S(2)}, u32[]{:S(2)}) %collective-permute-start.27) | collective-permute-done | bytes 196640 | tf_op jit(solution)/shard_map/ppermute | solution.py:20
  80.4 1.3 %collective-permute-start.35 = (bf16[96,1024]{1,0:T(8,128)(2,1)S(1)}, bf16[96,1024]{1,0:T(8,128)(2,1)S(1)}, u32[]{:S(2)}, u32[]{:S(2)}) collective-permute-start(bf16[96,1024]{1,0:T(8,128)(2,1)S(1)} %add_convert_fusion.4), channel_id=1, source_target_pairs={{0,2},{1,3},{2,0},{3,1},{4,6},{5,7},{6,4},{7,5},{8,10},{9,11},{10,... | collective-permute-start | bytes 589832 | tf_op jit(solution)/shard_map/ppermute | solution.py:20
  81.8 0.8 collective-permute-start.11
  82.6 5.2 %collective-permute-done.35 = bf16[96,1024]{1,0:T(8,128)(2,1)S(1)} collective-permute-done((bf16[96,1024]{1,0:T(8,128)(2,1)S(1)}, bf16[96,1024]{1,0:T(8,128)(2,1)S(1)}, u32[]{:S(2)}, u32[]{:S(2)}) %collective-permute-start.35) | collective-permute-done | bytes 196640 | tf_op jit(solution)/shard_map/ppermute | solution.py:20
  87.7 0.7 collective-permute-start.20
  88.5 0.7 collective-permute-start.28
  89.2 0.6 collective-permute-done.11
  89.8 4.7 %collective-permute-start.36 = (bf16[96,1024]{1,0:T(8,128)(2,1)S(1)}, bf16[96,1024]{1,0:T(8,128)(2,1)S(1)}, u32[]{:S(2)}, u32[]{:S(2)}) collective-permute-start(bf16[96,1024]{1,0:T(8,128)(2,1)S(1)} %add_convert_fusion.3), channel_id=1, source_target_pairs={{0,24},{1,29},{2,26},{3,31},{4,28},{5,25},{6,30},{7,27},{8,16},{9,... | collective-permute-start | bytes 589832 | tf_op jit(solution)/shard_map/ppermute | solution.py:30
  94.7 10.8 %collective-permute-done.28.refs_1_ = bf16[96,1024]{1,0:T(8,128)(2,1)S(1)} collective-permute-done((bf16[96,1024]{1,0:T(8,128)(2,1)S(1)}, bf16[96,1024]{1,0:T(8,128)(2,1)S(1)}, u32[]{:S(2)}, u32[]{:S(2)}) %collective-permute-start.28) | collective-permute-done | bytes 196640 | tf_op jit(solution)/shard_map/ppermute | solution.py:30
  105.5 1.5 %combine.2.refs_1_ = f32[256,1024]{1,0:T(8,128)S(1)} custom-call(s32[4]{0:T(128)S(1)} %pad_add_fusion.me_ref.at_ref, f32[4,256]{1,0:T(4,128)S(1)} %get-tuple-element.34.slot_ref, f32[4,256]{1,0:T(4,128)S(1)} %get-tuple-element.35.weight_ref, bf16[96,1024]{1,0:T(8,128)(2,1)S(1)} %collective-permute-done.20.refs_0_, ...), custom_call_target="tpu_custom_call" | custom-call | flops 301989888 | bytes 1048576 | tf_op jit(solution)/shard_map/combine/pallas_call | solution.py:316
  107.1 1.1 combine.3
  108.2 0.8 add_convert_fusion.1
  109.0 0.7 collective-permute-done.37
  109.7 0.8 add_convert_fusion
  (58 shorter events, 2.8 us)
Async XLA Ops:
  0.6 1.9 %collective-permute-start.4 = (bf16[256,512]{1,0:T(8,128)(2,1)}, bf16[256,512]{1,0:T(8,128)(2,1)S(1)}, u32[]{:S(2)}, u32[]{:S(2)}) collective-permute-start(bf16[256,512]{1,0:T(8,128)(2,1)} %own_hbm.1), channel_id=1, source_target_pairs={{0,1},{1,0},{2,3},{3,2},{4,5},{5,4},{6,7},{7,6},{8,9},{9,8},{10,11... | collective-permute-start | bytes 786440 | tf_op jit(solution)/shard_map/ppermute | solution.py:20
  2.6 35.8 %copy-start = (bf16[1,2048,896]{2,1,0:T(8,128)(2,1)S(1)}, bf16[1,2048,896]{2,1,0:T(8,128)(2,1)}, u32[]{:S(2)}) copy-start(bf16[1,2048,896]{2,1,0:T(8,128)(2,1)} %wg_ref.7) | copy-start | bytes 11010052
  2.6 35.8 %copy-start.1 = (bf16[1,2048,896]{2,1,0:T(8,128)(2,1)S(1)}, bf16[1,2048,896]{2,1,0:T(8,128)(2,1)}, u32[]{:S(2)}) copy-start(bf16[1,2048,896]{2,1,0:T(8,128)(2,1)} %wu_ref.7) | copy-start | bytes 11010052
  2.6 35.8 %copy-start.2 = (bf16[1,896,2048]{2,1,0:T(8,128)(2,1)S(1)}, bf16[1,896,2048]{2,1,0:T(8,128)(2,1)}, u32[]{:S(2)}) copy-start(bf16[1,896,2048]{2,1,0:T(8,128)(2,1)} %wd_ref.7) | copy-start | bytes 11010052
  2.6 35.8 %copy-start.3 = (f32[2048]{0:T(1024)S(1)}, f32[2048]{0:T(1024)}, u32[]{:S(2)}) copy-start(f32[2048]{0:T(1024)} %param.18) | copy-start | bytes 24580
  4.9 11.4 %collective-permute-start.5 = (bf16[96,1024]{1,0:T(8,128)(2,1)S(1)}, bf16[96,1024]{1,0:T(8,128)(2,1)S(1)}, u32[]{:S(2)}, u32[]{:S(2)}) collective-permute-start(bf16[96,1024]{1,0:T(8,128)(2,1)S(1)} %get-tuple-element.36), channel_id=1, source_target_pairs={{0,8},{1,13},{2,10},{3,15},{4,12},{5,9},{6,14},{7,11},{8,0},{9,5},... | collective-permute-start | bytes 589832 | tf_op jit(solution)/shard_map/ppermute | solution.py:30
  7.9 4.7 %collective-permute-start = (bf16[2,2,256]{2,1,0:T(2,128)(2,1)S(1)}, bf16[2,2,256]{2,1,0:T(2,128)(2,1)S(1)}, u32[]{:S(2)}, u32[]{:S(2)}) collective-permute-start(bf16[2,2,256]{2,1,0:T(2,128)(2,1)S(1)} %pad_maximum_fusion), channel_id=1, source_target_pairs={{0,4},{4,8},{8,12},{12,16},{16,20},{20,24},{24,28},{1,5},{5,9},{9,... | collective-permute-start | bytes 6152 | tf_op jit(solution)/shard_map/ppermute | solution.py:36
  15.5 8.4 %collective-permute-start.2 = (bf16[64,2048]{1,0:T(8,128)(2,1)S(1)}, bf16[64,2048]{1,0:T(8,128)(2,1)S(1)}, u32[]{:S(2)}, u32[]{:S(2)}) collective-permute-start(bf16[64,2048]{1,0:T(8,128)(2,1)S(1)} %get-tuple-element.33), channel_id=1, source_target_pairs={{0,1},{1,0},{2,3},{3,2},{4,5},{5,4},{6,7},{7,6},{8,9},{9,8},{10,11... | collective-permute-start | bytes 786440 | tf_op jit(solution)/shard_map/ppermute | solution.py:20
  15.6 8.9 %collective-permute-start.13 = (bf16[96,1024]{1,0:T(8,128)(2,1)S(1)}, bf16[96,1024]{1,0:T(8,128)(2,1)S(1)}, u32[]{:S(2)}, u32[]{:S(2)}) collective-permute-start(bf16[96,1024]{1,0:T(8,128)(2,1)S(1)} %get-tuple-element.41), channel_id=1, source_target_pairs={{0,0},{1,5},{2,2},{3,7},{4,4},{5,1},{6,6},{7,3},{8,8},{9,13},{10,1... | collective-permute-start | bytes 589832 | tf_op jit(solution)/shard_map/ppermute | solution.py:30
  16.3 8.7 %collective-permute-start.6 = (bf16[96,1024]{1,0:T(8,128)(2,1)S(1)}, bf16[96,1024]{1,0:T(8,128)(2,1)S(1)}, u32[]{:S(2)}, u32[]{:S(2)}) collective-permute-start(bf16[96,1024]{1,0:T(8,128)(2,1)S(1)} %collective-permute-done.5.refs_0_), channel_id=1, source_target_pairs={{0,2},{1,3},{2,0},{3,1},{4,6},{5,7},{6,4},{7,5},{8,10},{9,11},{10,... | collective-permute-start | bytes 589832 | tf_op jit(solution)/shard_map/ppermute | solution.py:20
  17.8 90.4 %collective-permute-start.1 = (bf16[64,2048]{1,0:T(8,128)(2,1)S(1)}, bf16[64,2048]{1,0:T(8,128)(2,1)S(1)}, u32[]{:S(2)}, u32[]{:S(2)}) collective-permute-start(bf16[64,2048]{1,0:T(8,128)(2,1)S(1)} %get-tuple-element.31), channel_id=1, source_target_pairs={{0,1},{1,0},{2,3},{3,2},{4,5},{5,4},{6,7},{7,6},{8,9},{9,8},{10,11... | collective-permute-start | bytes 786440 | tf_op jit(solution)/shard_map/ppermute | solution.py:20
  21.3 11.9 %collective-permute-start.21 = (bf16[96,1024]{1,0:T(8,128)(2,1)S(1)}, bf16[96,1024]{1,0:T(8,128)(2,1)S(1)}, u32[]{:S(2)}, u32[]{:S(2)}) collective-permute-start(bf16[96,1024]{1,0:T(8,128)(2,1)S(1)} %get-tuple-element.46), channel_id=1, source_target_pairs={{0,16},{1,21},{2,18},{3,23},{4,20},{5,17},{6,22},{7,19},{8,24},{9,... | collective-permute-start | bytes 589832 | tf_op jit(solution)/shard_map/ppermute | solution.py:30
  23.9 13.3 %collective-permute-start.7 = (bf16[96,1024]{1,0:T(8,128)(2,1)S(1)}, bf16[96,1024]{1,0:T(8,128)(2,1)S(1)}, u32[]{:S(2)}, u32[]{:S(2)}) collective-permute-start(bf16[96,1024]{1,0:T(8,128)(2,1)S(1)} %collective-permute-done.5.refs_0_), channel_id=1, source_target_pairs={{0,1},{1,0},{2,3},{3,2},{4,5},{5,4},{6,7},{7,6},{8,9},{9,8},{10,11... | collective-permute-start | bytes 589832 | tf_op jit(solution)/shard_map/ppermute | solution.py:20
  24.5 13.4 %collective-permute-start.14 = (bf16[96,1024]{1,0:T(8,128)(2,1)S(1)}, bf16[96,1024]{1,0:T(8,128)(2,1)S(1)}, u32[]{:S(2)}, u32[]{:S(2)}) collective-permute-start(bf16[96,1024]{1,0:T(8,128)(2,1)S(1)} %collective-permute-done.13.refs_0_), channel_id=1, source_target_pairs={{0,2},{1,3},{2,0},{3,1},{4,6},{5,7},{6,4},{7,5},{8,10},{9,11},{10,... | collective-permute-start | bytes 589832 | tf_op jit(solution)/shard_map/ppermute | solution.py:20
  25.0 13.4 %collective-permute-start.8 = (bf16[96,1024]{1,0:T(8,128)(2,1)S(1)}, bf16[96,1024]{1,0:T(8,128)(2,1)S(1)}, u32[]{:S(2)}, u32[]{:S(2)}) collective-permute-start(bf16[96,1024]{1,0:T(8,128)(2,1)S(1)} %collective-permute-done.6.refs_1_), channel_id=1, source_target_pairs={{0,1},{1,0},{2,3},{3,2},{4,5},{5,4},{6,7},{7,6},{8,9},{9,8},{10,11... | collective-permute-start | bytes 589832 | tf_op jit(solution)/shard_map/ppermute | solution.py:20
  33.2 9.3 %collective-permute-start.29 = (bf16[96,1024]{1,0:T(8,128)(2,1)S(1)}, bf16[96,1024]{1,0:T(8,128)(2,1)S(1)}, u32[]{:S(2)}, u32[]{:S(2)}) collective-permute-start(bf16[96,1024]{1,0:T(8,128)(2,1)S(1)} %get-tuple-element.51), channel_id=1, source_target_pairs={{0,24},{1,29},{2,26},{3,31},{4,28},{5,25},{6,30},{7,27},{8,16},{9,... | collective-permute-start | bytes 589832 | tf_op jit(solution)/shard_map/ppermute | solution.py:30
  37.2 6.2 %collective-permute-start.15 = (bf16[96,1024]{1,0:T(8,128)(2,1)S(1)}, bf16[96,1024]{1,0:T(8,128)(2,1)S(1)}, u32[]{:S(2)}, u32[]{:S(2)}) collective-permute-start(bf16[96,1024]{1,0:T(8,128)(2,1)S(1)} %collective-permute-done.13.refs_0_), channel_id=1, source_target_pairs={{0,1},{1,0},{2,3},{3,2},{4,5},{5,4},{6,7},{7,6},{8,9},{9,8},{10,11... | collective-permute-start | bytes 589832 | tf_op jit(solution)/shard_map/ppermute | solution.py:20
  37.8 6.9 %collective-permute-start.22 = (bf16[96,1024]{1,0:T(8,128)(2,1)S(1)}, bf16[96,1024]{1,0:T(8,128)(2,1)S(1)}, u32[]{:S(2)}, u32[]{:S(2)}) collective-permute-start(bf16[96,1024]{1,0:T(8,128)(2,1)S(1)} %collective-permute-done.21.refs_0_), channel_id=1, source_target_pairs={{0,2},{1,3},{2,0},{3,1},{4,6},{5,7},{6,4},{7,5},{8,10},{9,11},{10,... | collective-permute-start | bytes 589832 | tf_op jit(solution)/shard_map/ppermute | solution.py:20
  38.3 6.9 %collective-permute-start.16 = (bf16[96,1024]{1,0:T(8,128)(2,1)S(1)}, bf16[96,1024]{1,0:T(8,128)(2,1)S(1)}, u32[]{:S(2)}, u32[]{:S(2)}) collective-permute-start(bf16[96,1024]{1,0:T(8,128)(2,1)S(1)} %collective-permute-done.14.refs_1_), channel_id=1, source_target_pairs={{0,1},{1,0},{2,3},{3,2},{4,5},{5,4},{6,7},{7,6},{8,9},{9,8},{10,11... | collective-permute-start | bytes 589832 | tf_op jit(solution)/shard_map/ppermute | solution.py:20
  42.5 65.8 %collective-permute-start.3 = (bf16[64,2048]{1,0:T(8,128)(2,1)S(1)}, bf16[64,2048]{1,0:T(8,128)(2,1)S(1)}, u32[]{:S(2)}, u32[]{:S(2)}) collective-permute-start(bf16[64,2048]{1,0:T(8,128)(2,1)S(1)} %add_convert_fusion.2), channel_id=1, source_target_pairs={{0,2},{1,3},{2,0},{3,1},{4,6},{5,7},{6,4},{7,5},{8,10},{9,11},{10,... | collective-permute-start | bytes 786440 | tf_op jit(solution)/shard_map/ppermute | solution.py:20
  43.4 5.2 %collective-permute-start.23 = (bf16[96,1024]{1,0:T(8,128)(2,1)S(1)}, bf16[96,1024]{1,0:T(8,128)(2,1)S(1)}, u32[]{:S(2)}, u32[]{:S(2)}) collective-permute-start(bf16[96,1024]{1,0:T(8,128)(2,1)S(1)} %collective-permute-done.21.refs_0_), channel_id=1, source_target_pairs={{0,1},{1,0},{2,3},{3,2},{4,5},{5,4},{6,7},{7,6},{8,9},{9,8},{10,11... | collective-permute-start | bytes 589832 | tf_op jit(solution)/shard_map/ppermute | solution.py:20
  44.7 10.3 %collective-permute-start.30 = (bf16[96,1024]{1,0:T(8,128)(2,1)S(1)}, bf16[96,1024]{1,0:T(8,128)(2,1)S(1)}, u32[]{:S(2)}, u32[]{:S(2)}) collective-permute-start(bf16[96,1024]{1,0:T(8,128)(2,1)S(1)} %collective-permute-done.29.refs_0_), channel_id=1, source_target_pairs={{0,2},{1,3},{2,0},{3,1},{4,6},{5,7},{6,4},{7,5},{8,10},{9,11},{10,... | collective-permute-start | bytes 589832 | tf_op jit(solution)/shard_map/ppermute | solution.py:20
  45.2 9.8 %collective-permute-start.24 = (bf16[96,1024]{1,0:T(8,128)(2,1)S(1)}, bf16[96,1024]{1,0:T(8,128)(2,1)S(1)}, u32[]{:S(2)}, u32[]{:S(2)}) collective-permute-start(bf16[96,1024]{1,0:T(8,128)(2,1)S(1)} %collective-permute-done.22.refs_1_), channel_id=1, source_target_pairs={{0,1},{1,0},{2,3},{3,2},{4,5},{5,4},{6,7},{7,6},{8,9},{9,8},{10,11... | collective-permute-start | bytes 589832 | tf_op jit(solution)/shard_map/ppermute | solution.py:20
  48.6 10.3 %collective-permute-start.31 = (bf16[96,1024]{1,0:T(8,128)(2,1)S(1)}, bf16[96,1024]{1,0:T(8,128)(2,1)S(1)}, u32[]{:S(2)}, u32[]{:S(2)}) collective-permute-start(bf16[96,1024]{1,0:T(8,128)(2,1)S(1)} %collective-permute-done.29.refs_0_), channel_id=1, source_target_pairs={{0,1},{1,0},{2,3},{3,2},{4,5},{5,4},{6,7},{7,6},{8,9},{9,8},{10,11... | collective-permute-start | bytes 589832 | tf_op jit(solution)/shard_map/ppermute | solution.py:20
  55.0 4.0 %collective-permute-start.32 = (bf16[96,1024]{1,0:T(8,128)(2,1)S(1)}, bf16[96,1024]{1,0:T(8,128)(2,1)S(1)}, u32[]{:S(2)}, u32[]{:S(2)}) collective-permute-start(bf16[96,1024]{1,0:T(8,128)(2,1)S(1)} %collective-permute-done.30.refs_1_), channel_id=1, source_target_pairs={{0,1},{1,0},{2,3},{3,2},{4,5},{5,4},{6,7},{7,6},{8,9},{9,8},{10,11... | collective-permute-start | bytes 589832 | tf_op jit(solution)/shard_map/ppermute | solution.py:20
  55.0 33.5 %collective-permute-start.9 = (bf16[96,1024]{1,0:T(8,128)(2,1)S(1)}, bf16[96,1024]{1,0:T(8,128)(2,1)S(1)}, u32[]{:S(2)}, u32[]{:S(2)}) collective-permute-start(bf16[96,1024]{1,0:T(8,128)(2,1)S(1)} %get-tuple-element.38), channel_id=1, source_target_pairs={{0,1},{1,0},{2,3},{3,2},{4,5},{5,4},{6,7},{7,6},{8,9},{9,8},{10,11... | collective-permute-start | bytes 589832 | tf_op jit(solution)/shard_map/ppermute | solution.py:20
  59.0 4.0 %collective-permute-start.10 = (bf16[96,1024]{1,0:T(8,128)(2,1)S(1)}, bf16[96,1024]{1,0:T(8,128)(2,1)S(1)}, u32[]{:S(2)}, u32[]{:S(2)}) collective-permute-start(bf16[96,1024]{1,0:T(8,128)(2,1)S(1)} %get-tuple-element.40), channel_id=1, source_target_pairs={{0,1},{1,0},{2,3},{3,2},{4,5},{5,4},{6,7},{7,6},{8,9},{9,8},{10,11... | collective-permute-start | bytes 589832 | tf_op jit(solution)/shard_map/ppermute | solution.py:20
  59.0 9.7 %collective-permute-start.17 = (bf16[96,1024]{1,0:T(8,128)(2,1)S(1)}, bf16[96,1024]{1,0:T(8,128)(2,1)S(1)}, u32[]{:S(2)}, u32[]{:S(2)}) collective-permute-start(bf16[96,1024]{1,0:T(8,128)(2,1)S(1)} %get-tuple-element.43), channel_id=1, source_target_pairs={{0,1},{1,0},{2,3},{3,2},{4,5},{5,4},{6,7},{7,6},{8,9},{9,8},{10,11... | collective-permute-start | bytes 589832 | tf_op jit(solution)/shard_map/ppermute | solution.py:20
  63.0 1.5 %collective-permute-start.18 = (bf16[96,1024]{1,0:T(8,128)(2,1)S(1)}, bf16[96,1024]{1,0:T(8,128)(2,1)S(1)}, u32[]{:S(2)}, u32[]{:S(2)}) collective-permute-start(bf16[96,1024]{1,0:T(8,128)(2,1)S(1)} %get-tuple-element.45), channel_id=1, source_target_pairs={{0,1},{1,0},{2,3},{3,2},{4,5},{5,4},{6,7},{7,6},{8,9},{9,8},{10,11... | collective-permute-start | bytes 589832 | tf_op jit(solution)/shard_map/ppermute | solution.py:20
  64.5 1.4 %collective-permute-start.26 = (bf16[96,1024]{1,0:T(8,128)(2,1)S(1)}, bf16[96,1024]{1,0:T(8,128)(2,1)S(1)}, u32[]{:S(2)}, u32[]{:S(2)}) collective-permute-start(bf16[96,1024]{1,0:T(8,128)(2,1)S(1)} %get-tuple-element.50), channel_id=1, source_target_pairs={{0,1},{1,0},{2,3},{3,2},{4,5},{5,4},{6,7},{7,6},{8,9},{9,8},{10,11... | collective-permute-start | bytes 589832 | tf_op jit(solution)/shard_map/ppermute | solution.py:20
  65.9 1.4 %collective-permute-start.34 = (bf16[96,1024]{1,0:T(8,128)(2,1)S(1)}, bf16[96,1024]{1,0:T(8,128)(2,1)S(1)}, u32[]{:S(2)}, u32[]{:S(2)}) collective-permute-start(bf16[96,1024]{1,0:T(8,128)(2,1)S(1)} %get-tuple-element.55), channel_id=1, source_target_pairs={{0,1},{1,0},{2,3},{3,2},{4,5},{5,4},{6,7},{7,6},{8,9},{9,8},{10,11... | collective-permute-start | bytes 589832 | tf_op jit(solution)/shard_map/ppermute | solution.py:20
  67.3 6.9 %collective-permute-start.19 = (bf16[96,1024]{1,0:T(8,128)(2,1)S(1)}, bf16[96,1024]{1,0:T(8,128)(2,1)S(1)}, u32[]{:S(2)}, u32[]{:S(2)}) collective-permute-start(bf16[96,1024]{1,0:T(8,128)(2,1)S(1)} %add_convert_fusion.8), channel_id=1, source_target_pairs={{0,2},{1,3},{2,0},{3,1},{4,6},{5,7},{6,4},{7,5},{8,10},{9,11},{10,... | collective-permute-start | bytes 589832 | tf_op jit(solution)/shard_map/ppermute | solution.py:20
  68.7 7.0 %collective-permute-start.25 = (bf16[96,1024]{1,0:T(8,128)(2,1)S(1)}, bf16[96,1024]{1,0:T(8,128)(2,1)S(1)}, u32[]{:S(2)}, u32[]{:S(2)}) collective-permute-start(bf16[96,1024]{1,0:T(8,128)(2,1)S(1)} %get-tuple-element.48), channel_id=1, source_target_pairs={{0,1},{1,0},{2,3},{3,2},{4,5},{5,4},{6,7},{7,6},{8,9},{9,8},{10,11... | collective-permute-start | bytes 589832 | tf_op jit(solution)/shard_map/ppermute | solution.py:20
  74.3 6.1 %collective-permute-start.27 = (bf16[96,1024]{1,0:T(8,128)(2,1)S(1)}, bf16[96,1024]{1,0:T(8,128)(2,1)S(1)}, u32[]{:S(2)}, u32[]{:S(2)}) collective-permute-start(bf16[96,1024]{1,0:T(8,128)(2,1)S(1)} %add_convert_fusion.6), channel_id=1, source_target_pairs={{0,2},{1,3},{2,0},{3,1},{4,6},{5,7},{6,4},{7,5},{8,10},{9,11},{10,... | collective-permute-start | bytes 589832 | tf_op jit(solution)/shard_map/ppermute | solution.py:20
  75.7 6.1 %collective-permute-start.33 = (bf16[96,1024]{1,0:T(8,128)(2,1)S(1)}, bf16[96,1024]{1,0:T(8,128)(2,1)S(1)}, u32[]{:S(2)}, u32[]{:S(2)}) collective-permute-start(bf16[96,1024]{1,0:T(8,128)(2,1)S(1)} %get-tuple-element.53), channel_id=1, source_target_pairs={{0,1},{1,0},{2,3},{3,2},{4,5},{5,4},{6,7},{7,6},{8,9},{9,8},{10,11... | collective-permute-start | bytes 589832 | tf_op jit(solution)/shard_map/ppermute | solution.py:20
  80.4 7.3 %collective-permute-start.35 = (bf16[96,1024]{1,0:T(8,128)(2,1)S(1)}, bf16[96,1024]{1,0:T(8,128)(2,1)S(1)}, u32[]{:S(2)}, u32[]{:S(2)}) collective-permute-start(bf16[96,1024]{1,0:T(8,128)(2,1)S(1)} %add_convert_fusion.4), channel_id=1, source_target_pairs={{0,2},{1,3},{2,0},{3,1},{4,6},{5,7},{6,4},{7,5},{8,10},{9,11},{10,... | collective-permute-start | bytes 589832 | tf_op jit(solution)/shard_map/ppermute | solution.py:20
  81.8 8.1 %collective-permute-start.11 = (bf16[96,1024]{1,0:T(8,128)(2,1)S(1)}, bf16[96,1024]{1,0:T(8,128)(2,1)S(1)}, u32[]{:S(2)}, u32[]{:S(2)}) collective-permute-start(bf16[96,1024]{1,0:T(8,128)(2,1)S(1)} %add_convert_fusion.10), channel_id=1, source_target_pairs={{0,2},{1,3},{2,0},{3,1},{4,6},{5,7},{6,4},{7,5},{8,10},{9,11},{10,... | collective-permute-start | bytes 589832 | tf_op jit(solution)/shard_map/ppermute | solution.py:20
  87.7 6.9 %collective-permute-start.20 = (bf16[96,1024]{1,0:T(8,128)(2,1)S(1)}, bf16[96,1024]{1,0:T(8,128)(2,1)S(1)}, u32[]{:S(2)}, u32[]{:S(2)}) collective-permute-start(bf16[96,1024]{1,0:T(8,128)(2,1)S(1)} %add_convert_fusion.7), channel_id=1, source_target_pairs={{0,0},{1,5},{2,2},{3,7},{4,4},{5,1},{6,6},{7,3},{8,8},{9,13},{10,1... | collective-permute-start | bytes 589832 | tf_op jit(solution)/shard_map/ppermute | solution.py:30
  88.5 17.0 %collective-permute-start.28 = (bf16[96,1024]{1,0:T(8,128)(2,1)S(1)}, bf16[96,1024]{1,0:T(8,128)(2,1)S(1)}, u32[]{:S(2)}, u32[]{:S(2)}) collective-permute-start(bf16[96,1024]{1,0:T(8,128)(2,1)S(1)} %add_convert_fusion.5), channel_id=1, source_target_pairs={{0,16},{1,21},{2,18},{3,23},{4,20},{5,17},{6,22},{7,19},{8,24},{9,... | collective-permute-start | bytes 589832 | tf_op jit(solution)/shard_map/ppermute | solution.py:30
  89.8 15.7 %collective-permute-start.36 = (bf16[96,1024]{1,0:T(8,128)(2,1)S(1)}, bf16[96,1024]{1,0:T(8,128)(2,1)S(1)}, u32[]{:S(2)}, u32[]{:S(2)}) collective-permute-start(bf16[96,1024]{1,0:T(8,128)(2,1)S(1)} %add_convert_fusion.3), channel_id=1, source_target_pairs={{0,24},{1,29},{2,26},{3,31},{4,28},{5,25},{6,30},{7,27},{8,16},{9,... | collective-permute-start | bytes 589832 | tf_op jit(solution)/shard_map/ppermute | solution.py:30
  94.6 12.5 %collective-permute-start.12 = (bf16[96,1024]{1,0:T(8,128)(2,1)S(1)}, bf16[96,1024]{1,0:T(8,128)(2,1)S(1)}, u32[]{:S(2)}, u32[]{:S(2)}) collective-permute-start(bf16[96,1024]{1,0:T(8,128)(2,1)S(1)} %add_convert_fusion.9), channel_id=1, source_target_pairs={{0,8},{1,13},{2,10},{3,15},{4,12},{5,9},{6,14},{7,11},{8,0},{9,5},... | collective-permute-start | bytes 589832 | tf_op jit(solution)/shard_map/ppermute | solution.py:30
  108.1 1.6 %collective-permute-start.37 = (bf16[256,512]{1,0:T(8,128)(2,1)S(1)}, bf16[256,512]{1,0:T(8,128)(2,1)S(1)}, u32[]{:S(2)}, u32[]{:S(2)}) collective-permute-start(bf16[256,512]{1,0:T(8,128)(2,1)S(1)} %get-tuple-element.57), channel_id=1, source_target_pairs={{0,1},{1,0},{2,3},{3,2},{4,5},{5,4},{6,7},{7,6},{8,9},{9,8},{10,11... | collective-permute-start | bytes 786440 | tf_op jit(solution)/shard_map/ppermute | solution.py:20
